TPU v7x, 32 devices: a whole 2x2x4 slice. The times are simulated.
32 devices in a mesh: sp: 4 (over z), tp: 4 (over y, x), dp: 2 (over core).
Axes of the slice: x: 2, y: 2, z: 4, core: 2. Of those that a mesh axis runs over, the one named last changes fastest.
Arguments:
- latent: bfloat16 [2, 3072, 2048], P('dp', ('sp', 'tp')), may hold values from -3 to 3
- cond: bfloat16 [2, 2048], P('dp', 'sp'), may hold values from -6 to 6
- cond_ctx: bfloat16 [2048], P('sp'), may hold values from -6 to 6
- context: bfloat16 [2, 512, 2048], P('dp', 'sp'), may hold values from -6 to 6
- norm_gain: bfloat16 [2048], replicated, may hold values from 0.099609375 to 1.8984375
- mod_shift: bfloat16 [2048, 2048], P('sp', 'tp'), may hold values from -0.125 to 0.125
- mod_scale: bfloat16 [2048, 2048], P('sp', 'tp'), may hold values from -0.125 to 0.125
- mod_gate: bfloat16 [2048, 2048], P('sp', 'tp'), may hold values from -0.125 to 0.125
- w_query: bfloat16 [2048, 1024], P(None, 'tp'), may hold values from -0.125 to 0.125
- w_key: bfloat16 [2048, 256], P(None, 'tp'), may hold values from -0.125 to 0.125
- w_value: bfloat16 [2048, 256], P(None, 'tp'), may hold values from -0.125 to 0.125
- q_gain: bfloat16 [64], replicated, may hold values from 1 to 5.5
- k_gain: bfloat16 [64], replicated, may hold values from 1 to 5.5
- ctx_lift: float32 [16], P('tp'), may hold values from 1 to 3
- w_out: bfloat16 [1024, 2048], replicated, may hold values from -1.5 to 1.5
Outputs:
- mixed: bfloat16 [2, 3072, 2048], P('dp', ('sp', 'tp'))
All inputs are finite; a program needn't handle non-finite values.
Results may differ from a plain program's by a relative error of at most 0.009.
The roundings to bfloat16 on the way count: a program that leaves them out, or rounds other values in their place, can miss the bound.
Values may be sent and summed in bfloat16 or wider, within the bound.
A program may use at most 64 MiB of HBM per device.

v0:
```python
import jax
import jax.numpy as jnp
from jax import lax
from jax.sharding import PartitionSpec as P

HD = 64
GRID_W = 128


EPS = 1e-06
THETA = 10000.0


def modulate(row_block, gain_vec, shift_rows, scale_rows):
    values = row_block.astype(jnp.float32)
    normed = (
        values
        * lax.rsqrt(jnp.mean(values * values, axis=-1, keepdims=True) + EPS)
        * gain_vec.astype(jnp.float32)
    )
    return (normed * (1.0 + scale_rows) + shift_rows).astype(jnp.bfloat16)


def head_norm(raw_proj, gain_vec):
    samples, tokens, width = raw_proj.shape
    pieces = raw_proj.reshape(samples, tokens, width // HD, HD)
    normed = (
        pieces
        * lax.rsqrt(jnp.mean(pieces * pieces, axis=-1, keepdims=True) + EPS)
        * gain_vec.astype(jnp.float32)
    )
    return normed.transpose(0, 2, 1, 3)


def rotate(vector, positions):
    pairs_count = vector.shape[-1] // 4
    grid_row = (positions // GRID_W).astype(jnp.float32)
    grid_col = (positions % GRID_W).astype(jnp.float32)
    inverse = THETA ** (-jnp.arange(pairs_count, dtype=jnp.float32) / pairs_count)
    angles = jnp.concatenate([grid_row[:, None] * inverse, grid_col[:, None] * inverse], axis=-1)
    cosine = jnp.cos(angles)
    sine_val = jnp.sin(angles)
    first_half = vector[..., 0::2]
    second_half = vector[..., 1::2]
    turned = jnp.stack(
        [
            first_half * cosine - second_half * sine_val,
            first_half * sine_val + second_half * cosine,
        ],
        axis=-1,
    )
    return turned.reshape(vector.shape)


def split_heads(rows):
    samples, tokens, width = rows.shape
    return rows.reshape(samples, tokens, width // HD, HD).transpose(0, 2, 1, 3)


def on_device(
    latent,
    cond,
    cond_ctx,
    context,
    norm_gain,
    mod_shift,
    mod_scale,
    mod_gate,
    w_query,
    w_key,
    w_value,
    q_gain,
    k_gain,
    ctx_lift,
    w_out,
):
    samples = latent.shape[0]
    active = jax.nn.silu(
        jnp.concatenate([cond, cond_ctx[None, :]], axis=0).astype(jnp.float32)
    ).astype(jnp.bfloat16)
    partial_mods = tuple(
        (
            jnp.dot(active, weight, preferred_element_type=jnp.float32)
            for weight in (mod_shift, mod_scale, mod_gate)
        )
    )
    summed = lax.psum(partial_mods, "sp")
    shift_rows, scale_rows, gate_rows = lax.all_gather(summed, "tp", axis=1, tiled=True)
    modulated = modulate(
        latent, norm_gain, shift_rows[:samples, None, :], scale_rows[:samples, None, :]
    )
    ctx_mod = modulate(context, norm_gain, shift_rows[samples], scale_rows[samples])
    q_width = w_query.shape[1]
    k_width = w_key.shape[1]
    w_joint = jnp.concatenate([w_query, w_key, w_value], axis=1)
    projected = jnp.einsum(
        "srd,dc->src",
        lax.all_gather(modulated, "tp", axis=1, tiled=True),
        w_joint,
        preferred_element_type=jnp.float32,
    )
    tokens = projected.shape[1]
    k_heads = k_width // HD
    group_size = q_width // k_width
    positions = lax.axis_index("sp") * tokens + jnp.arange(tokens, dtype=jnp.int32)
    queries = rotate(head_norm(projected[..., :q_width], q_gain), positions).astype(jnp.bfloat16)
    queries = queries.reshape(samples, k_heads, group_size, tokens, HD)
    key_rows = rotate(
        head_norm(projected[..., q_width : q_width + k_width], k_gain), positions
    ).astype(jnp.bfloat16)
    value_rows = split_heads(projected[..., q_width + k_width :].astype(jnp.bfloat16))
    ctx_proj = jnp.einsum(
        "srd,dc->src", ctx_mod, w_joint[:, q_width:], preferred_element_type=jnp.float32
    )
    ctx_keys = head_norm(ctx_proj[..., :k_width], k_gain).astype(jnp.bfloat16)
    ctx_values = split_heads(ctx_proj[..., k_width:].astype(jnp.bfloat16))
    lift_table = ctx_lift.reshape(1, k_heads, group_size, 1, 1)
    factor = HD ** (-0.5)

    def absorb(state_now, key_block, value_block, score_lift):
        best_old, weight_sum, accumulated = state_now
        scores = (
            jnp.einsum("skgtd,skrd->skgtr", queries, key_block, preferred_element_type=jnp.float32)
            * factor
            + score_lift
        )
        peak = jnp.maximum(best_old, jnp.max(scores, axis=-1))
        weights = jnp.exp(scores - peak[..., None])
        rescale = jnp.exp(best_old - peak)
        weight_sum = weight_sum * rescale + jnp.sum(weights, axis=-1)
        accumulated = accumulated * rescale[..., None] + jnp.einsum(
            "skgtr,skrd->skgtd",
            weights.astype(jnp.bfloat16),
            value_block,
            preferred_element_type=jnp.float32,
        )
        return (peak, weight_sum, accumulated)

    stat_shape = (samples, k_heads, group_size, tokens)
    state_now = (
        jnp.full(stat_shape, -1e30, jnp.float32),
        jnp.zeros(stat_shape, jnp.float32),
        jnp.zeros(stat_shape + (HD,), jnp.float32),
    )
    all_ctx_keys, all_ctx_values = (
        lax.all_gather(ctx_keys, "sp", axis=2, tiled=True),
        lax.all_gather(ctx_values, "sp", axis=2, tiled=True),
    )
    state_now = absorb(state_now, all_ctx_keys, all_ctx_values, lift_table)
    key_piece = lax.all_gather(key_rows, "sp", axis=2, tiled=True)
    value_piece = lax.all_gather(value_rows, "sp", axis=2, tiled=True)
    block_count = key_piece.shape[2] // tokens
    key_blocks = jnp.moveaxis(key_piece.reshape(samples, k_heads, block_count, tokens, HD), 2, 0)
    value_blocks = jnp.moveaxis(
        value_piece.reshape(samples, k_heads, block_count, tokens, HD), 2, 0
    )

    def step_block(carry, blocks):
        return (absorb(carry, blocks[0], blocks[1], 0.0), None)

    state_out, unused = lax.scan(step_block, state_now, (key_blocks, value_blocks))
    state_now = state_out
    best_old, weight_sum, accumulated = state_now
    attended = (accumulated / weight_sum[..., None]).astype(jnp.bfloat16)
    head_rows = attended.transpose(0, 3, 1, 2, 4).reshape(samples, tokens, q_width)
    projected_out = jnp.einsum(
        "srq,qd->srd",
        lax.all_to_all(head_rows, "tp", split_axis=1, concat_axis=2, tiled=True),
        w_out,
        preferred_element_type=jnp.float32,
    )
    return (latent.astype(jnp.float32) + gate_rows[:samples, None, :] * projected_out).astype(
        jnp.bfloat16
    )


def solution(mesh):
    placed = (
        P("dp", ("sp", "tp"), None),
        P("dp", "sp"),
        P("sp"),
        P("dp", "sp", None),
        P(),
        P("sp", "tp"),
        P("sp", "tp"),
        P("sp", "tp"),
        P(None, "tp"),
        P(None, "tp"),
        P(None, "tp"),
        P(),
        P(),
        P("tp"),
        P(),
    )
    return jax.shard_map(
        on_device,
        mesh=mesh,
        in_specs=placed,
        out_specs=P("dp", ("sp", "tp"), None),
        check_vma=False,
    )
```

profile of v0, /device:TPU:0, one launch (start us, length us, event | category | flops | bytes accessed | tf_op | source)
XLA Modules:
  0.0 190.3 jit_solution(14167755606228791362)
XLA Ops:
  6.6 0.8 broadcast_in_dim.10
  7.4 0.2 copy-done
  7.6 0.8 fusion.94
  8.4 1.2 fusion.96
  9.7 1.2 fusion.98
  10.9 20.5 %all-reduce = (f32[2,512]{1,0:T(2,128)S(1)}, f32[2,512]{1,0:T(2,128)S(1)}, f32[2,512]{1,0:T(2,128)S(1)}) all-reduce(f32[2,512]{1,0:T(2,128)S(1)} %fusion.94, f32[2,512]{1,0:T(2,128)S(1)} %fusion.96, f32[2,512]{1,0:T(2,128)S(1)} %fusion.98), channel_id=1, replica_groups=mesh['sp'=4,'tp'=4,'dp'=2] {'sp'}, use_global_device_ids=true, to_apply=%region_3.4 | all-reduce | flops 3072 | bytes 24576 | tf_op jit(solution)/shard_map/psum | solution.py:87
  31.4 8.2 %all_gather.25 = f32[2,2048]{1,0:T(2,128)S(1)} all-gather(f32[2,512]{1,0:T(2,128)S(1)} %get-tuple-element.88), channel_id=1, replica_groups=mesh['sp'=4,'tp'=4,'dp'=2] {'tp'}, dimensions={1}, use_global_device_ids=true | all-gather | bytes 20480 | tf_op jit(solution)/shard_map/all_gather | solution.py:88
  39.6 8.2 %all_gather.26 = f32[2,2048]{1,0:T(2,128)S(1)} all-gather(f32[2,512]{1,0:T(2,128)S(1)} %get-tuple-element.87), channel_id=1, replica_groups=mesh['sp'=4,'tp'=4,'dp'=2] {'tp'}, dimensions={1}, use_global_device_ids=true | all-gather | bytes 20480 | tf_op jit(solution)/shard_map/all_gather | solution.py:88
  47.7 0.7 convert_element_type.119
  48.4 1.4 fusion.31
  49.8 2.4 %fusion.35 = bf16[1,192,2048]{2,1,0:T(8,128)(2,1)} fusion(bf16[1,192,2048]{2,1,0:T(8,128)(2,1)} %param.17, f32[2048]{0:T(1024)S(1)} %bitcast.173, f32[2048]{0:T(1024)S(1)} %bitcast.172, f32[2048]{0:T(1024)S(1)} %convert_element_type.119, f32[192]{0:T(256)S(1)} %add_rsqrt_fusion.2), kind=kLoop, calls=%fused_computation.39 | loop fusion | flops 2359296 | bytes 1598208 | tf_op jit(solution)/shard_map/convert_element_type | solution.py:21
  52.2 0.3 copy.46
  52.5 0.3 copy.47
  52.9 0.2 fusion.52
  53.1 0.4 convolution_bitcast_fusion
  53.6 0.1 fusion.77
  53.6 12.0 %all_gather.28 = bf16[1,1,512,64]{2,3,1,0:T(8,128)(2,1)S(1)} all-gather(bf16[1,1,128,64]{2,3,1,0:T(8,128)(2,1)S(1)} %fusion.77), channel_id=1, replica_groups=mesh['sp'=4,'tp'=4,'dp'=2] {'sp'}, dimensions={2}, use_global_device_ids=true | all-gather | bytes 81920 | tf_op jit(solution)/shard_map/all_gather | solution.py:146
  65.7 12.6 %all-gather = bf16[1,512,64]{1,2,0:T(8,128)(2,1)} all-gather(bf16[1,128,64]{1,2,0:T(8,128)(2,1)S(1)} %slice.80), channel_id=2, replica_groups=mesh['sp'=4,'tp'=4,'dp'=2] {'sp'}, dimensions={1}, use_global_device_ids=true | all-gather | bytes 81920 | tf_op jit(solution)/shard_map/all_gather | solution.py:147
  78.3 0.7 fusion.78
  79.0 1.0 fusion.70
  80.1 13.4 %all-gather.4.cloned.1.call-done = bf16[1,768,2048]{2,1,0:T(8,128)(2,1)} async-done(((bf16[1,192,2048]{2,1,0:T(8,128)(2,1)}), bf16[1,768,2048]{2,1,0:T(8,128)(2,1)}) %all-gather.4.cloned.1.call-update) | async-done | bytes 3145744 | tf_op jit(solution)/shard_map/all_gather | solution.py:98
  93.5 3.7 %fusion.41 = f32[1,768,384]{1,2,0:T(8,128)S(1)} fusion(bf16[2048,64]{1,0:T(8,128)(2,1)S(1)} %copy.47, bf16[2048,64]{1,0:T(8,128)(2,1)S(1)} %copy.46, bf16[2048,256]{1,0:T(8,128)(2,1)} %param.25, bf16[1,768,2048]{2,1,0:T(8,128)(2,1)} %all-gather.4.cloned.1.call-done), kind=kOutput, calls=%fused_computation.45 | convolution fusion | flops 1212678144 | bytes 5898240 | tf_op jit(solution)/shard_map/srd,dc->src/dot_general | solution.py:96
  97.2 0.1 fusion.66
  97.4 0.1 multiply_reduce_fusion
  97.5 0.1 multiply_bitcast_fusion
  97.7 0.2 slice.50
  97.9 0.2 slice.51
  98.1 1.0 subtract_bitcast_fusion
  99.2 0.4 copy.48
  99.6 0.1 convert_element_type.125
  99.7 0.1 convert_element_type.132
  99.9 1.2 fusion.74
  101.1 0.1 copy.50
  101.3 14.6 %all_gather.30 = bf16[1,1,3072,64]{2,3,1,0:T(8,128)(2,1)S(1)} all-gather(bf16[1,1,768,64]{2,3,1,0:T(8,128)(2,1)S(1)} %convert_element_type.131), channel_id=1, replica_groups=mesh['sp'=4,'tp'=4,'dp'=2] {'sp'}, dimensions={2}, use_global_device_ids=true | all-gather | bytes 491520 | tf_op jit(solution)/shard_map/all_gather | solution.py:150
  115.9 1.1 fusion.21
  117.0 2.6 %copy-done.1 = f32[4,768,512]{1,2,0:T(8,128)} copy-done((f32[4,768,512]{1,2,0:T(8,128)}, f32[4,768,512]{1,2,0:T(8,128)S(1)}, u32[]{:S(2)}) %copy-start.1) | copy-done | bytes 6291480
  119.6 1.3 fusion.23
  120.9 15.5 %all-gather.1 = bf16[1,3072,64]{1,2,0:T(8,128)(2,1)S(1)} all-gather(bf16[1,768,64]{1,2,0:T(8,128)(2,1)S(1)} %slice.79), channel_id=3, replica_groups=mesh['sp'=4,'tp'=4,'dp'=2] {'sp'}, dimensions={1}, use_global_device_ids=true | all-gather | bytes 491520 | tf_op jit(solution)/shard_map/all_gather | solution.py:151
  136.4 0.3 transpose_reshape.15
  136.8 4.3 %fusion.49 = f32[1,1,4,768,64]{3,4,2,1,0:T(8,128)S(1)} fusion(f32[4,768,512]{1,2,0:T(8,128)} %copy-done.1, f32[4,768]{1,0:T(4,128)S(1)} %get-tuple-element.106, f32[4]{0:T(128)S(1)} %copy-done.7, f32[4,768]{1,0:T(4,128)S(1)} %get-tuple-element.104, bf16[1,512,64]{1,2,0:T(8,128)(2,1)S(1)} %copy-done.6), kind=kOutput, calls=%fused_computation.49 | convolution fusion | flops 207814656 | bytes 7168016 | tf_op jit(solution)/shard_map/skgtr,skrd->skgtd/dot_general | solution.py:131
  141.0 19.7 %while.14 = (s32[]{:T(128)}, f32[1,1,4,768]{3,2,1,0:T(4,128)S(1)}, f32[1,1,4,768]{3,2,1,0:T(4,128)S(1)}, f32[1,1,4,768,64]{3,4,2,1,0:T(8,128)S(1)}, bf16[4,1,1,7...) while((s32[]{:T(128)}, f32[1,1,4,768]{3,2,1,0:T(4,128)S(1)}, ...), condition=%wide.region_13.14_spmd, body=%wide.region_10.13_spmd.sunk | while | flops 623256576 | bytes 30670940 | solution.py:161
  141.1 1.4 bitcast_reduce_fusion.2
  142.5 1.9 fusion.116
  144.4 1.6 fusion.115
  146.0 1.4 bitcast_reduce_fusion.2
  147.4 1.9 fusion.116
  149.3 1.6 fusion.115
  150.9 1.4 bitcast_reduce_fusion.2
  152.4 1.9 fusion.116
  154.3 1.6 fusion.115
  155.9 1.4 bitcast_reduce_fusion.2
  157.3 1.9 fusion.116
  159.2 1.6 fusion.115
  160.8 0.1 divide_convert_fusion
  160.9 0.6 copy.54
  161.5 0.5 broadcast.433
  162.0 3.0 %reduce.15 = bf16[768,256]{1,0:T(8,128)(2,1)S(1)} reduce(bf16[768,1,256]{2,1,0:T(2,128)(2,1)S(1)} %bitcast.162, bf16[]{:T(256)} %broadcast.433), dimensions={1}, to_apply=%bitcast.124.reduce_sub_computation | reduce | bytes 786434
  165.0 0.8 reshape.683
  165.9 3.5 %all-to-all-start = ((bf16[4,2,24576]{2,1,0:T(2,128)(2,1)}), bf16[4,2,24576]{2,1,0:T(2,128)(2,1)S(1)}, u32[]{:S(2)}, u32[]{:S(2)}) async-start(bf16[4,2,24576]{2,1,0:T(2,128)(2,1)} %reshape.683), calls=%async_computation | async-start | bytes 786432 | tf_op jit(solution)/shard_map/all_to_all | solution.py:168
  169.4 9.1 %all_gather.24 = f32[2,2048]{1,0:T(2,128)S(1)} all-gather(f32[2,512]{1,0:T(2,128)S(1)} %get-tuple-element.89), channel_id=1, replica_groups=mesh['sp'=4,'tp'=4,'dp'=2] {'tp'}, dimensions={1}, use_global_device_ids=true | all-gather | bytes 20480 | tf_op jit(solution)/shard_map/all_gather | solution.py:88
  178.4 0.4 reshape.684
  178.9 0.1 copy.58
  178.9 0.3 copy.55
  179.3 4.1 %fusion.30 = bf16[1,192,2048]{2,1,0:T(8,128)(2,1)} fusion(bf16[192,1024]{1,0:T(8,128)(2,1)S(1)} %bitcast.171, bf16[1024,2048]{1,0:T(8,128)(2,1)} %param.31, bf16[1,192,2048]{2,1,0:T(8,128)(2,1)S(1)} %copy-done.2, f32[2048]{0:T(1024)S(1)} %bitcast.174), kind=kOutput, calls=%fused_computation.32 | convolution fusion | flops 806879232 | bytes 6168576 | tf_op jit(solution)/shard_map/srq,qd->srd/dot_general | solution.py:166
  (60 shorter events, 0.8 us)
Async XLA Ops:
  6.5 1.0 copy-start
  6.5 45.7 %copy-start.5 = (bf16[2048,64]{0,1:T(8,128)(2,1)S(1)}, bf16[2048,64]{0,1:T(8,128)(2,1)}, u32[]{:S(2)}) copy-start(bf16[2048,64]{0,1:T(8,128)(2,1)} %param.26) | copy-start | bytes 786436
  6.5 46.0 %copy-start.4 = (bf16[2048,64]{0,1:T(8,128)(2,1)S(1)}, bf16[2048,64]{0,1:T(8,128)(2,1)}, u32[]{:S(2)}) copy-start(bf16[2048,64]{0,1:T(8,128)(2,1)} %param.27) | copy-start | bytes 786436
  6.5 46.3 %copy-start.8 = (bf16[64]{0:T(256)(128)(2,1)S(1)}, bf16[64]{0:T(256)(128)(2,1)}, u32[]{:S(2)}) copy-start(bf16[64]{0:T(256)(128)(2,1)} %param.29) | copy-start | bytes 388
  6.5 46.3 %copy-start.9 = (bf16[64]{0:T(256)(128)(2,1)S(1)}, bf16[64]{0:T(256)(128)(2,1)}, u32[]{:S(2)}) copy-start(bf16[64]{0:T(256)(128)(2,1)} %param.28) | copy-start | bytes 388
  6.5 46.3 %copy-start.3 = (bf16[1,128,2048]{2,1,0:T(8,128)(2,1)S(1)}, bf16[1,128,2048]{2,1,0:T(8,128)(2,1)}, u32[]{:S(2)}) copy-start(bf16[1,128,2048]{2,1,0:T(8,128)(2,1)} %param.20) | copy-start | bytes 1572868
  6.6 86.9 %all-gather.4.cloned.1.call-start = ((), (), s32[]{:S(2)}) async-start(), calls=%async_computation.1 | async-start | bytes 3932160 | tf_op jit(solution)/shard_map/all_gather | solution.py:98
  97.5 18.4 %copy-start.7 = (f32[4]{0:T(128)S(1)}, f32[4]{0:T(128)}, u32[]{:S(2)}) copy-start(f32[4]{0:T(128)} %param.30) | copy-start | bytes 52
  116.9 2.7 %copy-start.1 = (f32[4,768,512]{1,2,0:T(8,128)}, f32[4,768,512]{1,2,0:T(8,128)S(1)}, u32[]{:S(2)}) copy-start(f32[4,768,512]{1,2,0:T(8,128)S(1)} %get-tuple-element.114) | copy-start | bytes 18874372
  117.0 19.8 %copy-start.6 = (bf16[1,512,64]{1,2,0:T(8,128)(2,1)S(1)}, bf16[1,512,64]{1,2,0:T(8,128)(2,1)}, u32[]{:S(2)}) copy-start(bf16[1,512,64]{1,2,0:T(8,128)(2,1)} %all-gather) | copy-start | bytes 196612
  160.8 18.5 %copy-start.2 = (bf16[1,192,2048]{2,1,0:T(8,128)(2,1)S(1)}, bf16[1,192,2048]{2,1,0:T(8,128)(2,1)}, u32[]{:S(2)}) copy-start(bf16[1,192,2048]{2,1,0:T(8,128)(2,1)} %param.17) | copy-start | bytes 2359300
  165.9 12.5 %all-to-all-start = ((bf16[4,2,24576]{2,1,0:T(2,128)(2,1)}), bf16[4,2,24576]{2,1,0:T(2,128)(2,1)S(1)}, u32[]{:S(2)}, u32[]{:S(2)}) async-start(bf16[4,2,24576]{2,1,0:T(2,128)(2,1)} %reshape.683), calls=%async_computation | async-start | bytes 786432 | tf_op jit(solution)/shard_map/all_to_all | solution.py:168
Sparse Core Ops, SparseCore 0:
  52.3 41.0 all-gather.3
where the time goes:
time: 191 us; the launch traced here: 190 us
  blocking collectives  101 us (53%)
  matrix products  30 us (16%)
  other arithmetic  20 us (10%)
  between operations  13.8 us (7%)
  waiting for transfers between devices  13.4 us (7%)
  local copies, waits for them, and re-layouts  8.75 us (5%)
  starting transfers between devices  3.5 us (2%)
    all_gather x3, blocking collectives, on_device(): lax.all_gather(summed, 'tp', axis=1, tiled=True)  25.4 us
    psum x1, blocking collectives, on_device(): summed = lax.psum(partial_mods, 'sp')  20.5 us
    all_gather x1, blocking collectives, on_device(): value_piece = lax.all_gather(value_rows, 'sp', axis=2, tiled=True)  15.5 us
    all_gather x1, blocking collectives, on_device(): key_piece = lax.all_gather(key_rows, 'sp', axis=2, tiled=True)  14.6 us
    all_gather x1, waiting for transfers between devices, on_device(): lax.all_gather(modulated, 'tp', axis=1, tiled=True)  13.4 us
    all_gather x1, blocking collectives, on_device(): lax.all_gather(ctx_values, 'sp', axis=2, tiled=True)  12.6 us
    all_gather x1, blocking collectives, on_device(): lax.all_gather(ctx_keys, 'sp', axis=2, tiled=True)  12 us
    dot_general x5, matrix products, absorb(): jnp.einsum('skgtr,skrd->skgtd', weights.astype(jnp.bfloat16), value_block...  11.7 us
  transfers between devices with their start and end apart: 2, of which 1 were waited for; matrix products, arithmetic and copies ran while one was open for 2% of the time, Pallas kernels for 0%

commit v1 on v0

v1 whole, which is shorter than its diff:
```python
import functools

import jax
import jax.numpy as jnp
import numpy as np
from jax import lax
from jax.experimental import pallas as pl
from jax.experimental.pallas import tpu as pltpu
from jax.sharding import PartitionSpec as P

HD = 64
GRID_W = 128
EPS = 1e-06
THETA = 10000.0
MESH = pl.DeviceIdType.MESH
LOG2E = 1.4426950408889634


def rope_tables(grid_rows):
    n = HD // 4
    inverse = (np.float32(THETA) ** (-np.arange(n, dtype=np.float32) / np.float32(n))).astype(np.float32)

    def table(count, low):
        angles = (np.arange(count, dtype=np.float32)[:, None] * inverse).astype(np.float32)
        zero = np.zeros((count, 2 * n), np.float32)
        sign = np.tile(np.array([-1.0, 1.0], np.float32), n)
        c = np.repeat(np.cos(angles.astype(np.float64)), 2, axis=1).astype(np.float32)
        s = np.repeat(np.sin(angles.astype(np.float64)), 2, axis=1).astype(np.float32) * sign
        parts = ([c, zero], [s, zero]) if low else ([zero, c], [zero, s])
        return [np.tile(np.concatenate(p, axis=1), (1, 2)) for p in parts]

    return np.stack(table(grid_rows, True)), np.stack(table(GRID_W, False))


def kernel(
    n_sp, n_tp, group,
    latent, cond, cond_ctx, norm_gain, q_gain, k_gain, lift, row_tab, col_tab,
    context_h, mshift_h, mscale_h, mgate_h, wq_h, wk_h, wv_h, wout_h,
    out,
    context, mods_w, wq, wk, wv, wkv, wout,
    raw, part, part_in, mods_all, ab, rope, q_all, kv_all, acc, m_st, l_st, o_send, o_all,
    local_sem, lat_send, lat_recv, pa_send, pa_recv, pb_send, pb_recv, kv_send, kv_recv, o_ssem, o_rsem,
):
    rows = latent.shape[0]
    half = rows // 2
    width = latent.shape[1]
    chunk = width // n_tp
    tokens = rows * n_tp
    ctx_rows = context.shape[0]
    sp = lax.axis_index("sp")
    tp = lax.axis_index("tp")
    tx, ty = tp % 2, tp // 2
    peers = (ty * 2 + (1 - tx), (1 - ty) * 2 + tx, (1 - ty) * 2 + (1 - tx))
    sp_order = sorted(range(1, n_sp), key=lambda d: min(d, n_sp - d))

    local = [
        pltpu.make_async_copy(src, dst, local_sem.at[i])
        for i, (src, dst) in enumerate(
            (
                (mshift_h, mods_w.at[0]),
                (mscale_h, mods_w.at[1]),
                (mgate_h, mods_w.at[2]),
                (context_h, context),
                (wk_h, wk),
                (wv_h, wv),
                (wq_h, wq),
                (wout_h, wout),
            )
        )
    ]
    for copy in local:
        copy.start()

    barrier = pltpu.get_barrier_semaphore()
    for peer in peers:
        pl.semaphore_signal(barrier, inc=1, device_id={"tp": peer}, device_id_type=MESH)
    for d in range(1, n_sp):
        pl.semaphore_signal(barrier, inc=1, device_id={"sp": (sp + d) % n_sp}, device_id_type=MESH)
    pl.semaphore_wait(barrier, n_tp - 1 + n_sp - 1)

    def send(src, dst, ssem, rsem, device):
        return pltpu.make_async_remote_copy(
            src_ref=src, dst_ref=dst, send_sem=ssem, recv_sem=rsem, device_id=device, device_id_type=MESH
        )

    top, low = pl.ds(0, half), pl.ds(half, half)
    lat = []

    def send_rows(index, src, slot, piece, peer):
        copy = send(src, raw.at[slot, piece], lat_send.at[index], lat_recv.at[index], {"tp": peer})
        copy.start()
        lat.append(copy)

    send_rows(0, latent.at[top], 0, top, peers[0])
    send_rows(1, latent.at[low], 1, low, peers[1])
    send_rows(2, latent.at[low], 0, low, peers[0])
    send_rows(3, latent.at[top], 1, top, peers[1])

    act = jnp.concatenate([cond[...], cond_ctx[...]], axis=0).astype(jnp.float32)
    act = (act / (1.0 + jnp.exp(-act))).astype(jnp.bfloat16)
    act = jnp.concatenate([act, jnp.zeros((14, act.shape[1]), jnp.bfloat16)], axis=0)
    for i in range(3):
        local[i].wait()
    sums = [jnp.dot(act, mods_w[i], preferred_element_type=jnp.float32)[0:2] for i in range(3)]
    part[...] = jnp.concatenate(sums + [jnp.zeros((2, chunk), jnp.float32)], axis=0)
    pa = []
    for d in sp_order:
        copy = send(part, part_in.at[d - 1], pa_send.at[d - 1], pa_recv.at[d - 1], {"sp": (sp + d) % n_sp})
        copy.start()
        pa.append(copy)

    groups = tokens // GRID_W
    for i in range(2):
        for g in range(groups):
            rope[i, pl.ds(g * GRID_W, GRID_W), :] = (
                row_tab[i, pl.ds(sp * groups + g, 1), :] + col_tab[i, :, :]
            )
    local[4].wait()
    local[5].wait()
    wkv[...] = jnp.concatenate([wk[...], wv[...]], axis=1)

    total = part[...]
    for copy in pa:
        copy.wait_recv()
    for d in range(1, n_sp):
        total = total + part_in[d - 1]
    mods_all[tp] = total
    pb = []
    for i, peer in enumerate(peers):
        copy = send(mods_all.at[tp], mods_all.at[tp], pb_send.at[i], pb_recv.at[i], {"tp": peer})
        copy.start()
        pb.append(copy)
    lat[0].wait_recv()
    send_rows(4, raw.at[0, top], 2, top, peers[1])
    lat[1].wait_recv()
    send_rows(5, raw.at[1, low], 2, low, peers[0])

    for copy in pb:
        copy.wait_recv()
    gain = norm_gain[...].astype(jnp.float32)
    for j in range(n_tp):
        cols = pl.ds(j * chunk, chunk)
        block = mods_all[j]
        ab[0:2, cols] = gain[:, j * chunk : (j + 1) * chunk] * (1.0 + block[2:4])
        ab[2:4, cols] = block[0:2]

    lane = lax.broadcasted_iota(jnp.int32, (1, 2 * HD), 1)
    even = lane % 2 == 0
    left = lane < HD
    ones = (
        (lax.broadcasted_iota(jnp.int32, (2 * HD, 2 * HD), 0) < HD)
        == (lax.broadcasted_iota(jnp.int32, (2 * HD, 2 * HD), 1) < HD)
    ).astype(jnp.bfloat16)
    qg = jnp.concatenate([q_gain[...]] * 2, axis=1).astype(jnp.float32)
    kg = jnp.concatenate([k_gain[...]] * 2, axis=1).astype(jnp.float32)

    def modulated(block, row):
        values = block.astype(jnp.float32)
        scale = lax.rsqrt(jnp.mean(values * values, axis=-1, keepdims=True) + EPS)
        return (values * scale * ab[row : row + 1, :] + ab[row + 2 : row + 3, :]).astype(jnp.bfloat16)

    def headed(x, g):
        square = x * x
        high = square.astype(jnp.bfloat16)
        rest = (square - high.astype(jnp.float32)).astype(jnp.bfloat16)
        mean = (
            jnp.dot(high, ones, preferred_element_type=jnp.float32)
            + jnp.dot(rest, ones, preferred_element_type=jnp.float32)
        ) * (1.0 / HD)
        return x * lax.rsqrt(mean + EPS) * g

    def turned(x, cosine, sine):
        partner = jnp.where(even, pltpu.roll(x, 2 * HD - 1, 1), pltpu.roll(x, 1, 1))
        return x * cosine + partner * sine

    def absorb_rows(block, owner):
        u = modulated(block, 0)
        where = pl.ds(pl.multiple_of(owner * rows, rows), rows)
        cosine, sine = rope[0, where, :], rope[1, where, :]
        kv = jnp.dot(u, wkv[...], preferred_element_type=jnp.float32)
        keys = turned(headed(kv, kg), cosine, sine)
        kv_all[0, where, :] = jnp.where(left, keys, kv).astype(jnp.bfloat16)
        raw_q = jnp.dot(u, wq[...], preferred_element_type=jnp.float32)
        for pair in range(group // 2):
            x = raw_q[:, pair * 2 * HD : (pair + 1) * 2 * HD]
            x = turned(headed(x, qg), cosine, sine)
            q_all[owner * group + 2 * pair] = jnp.where(left, x, 0.0).astype(jnp.bfloat16)
            x = pltpu.roll(x, HD, 1)
            q_all[owner * group + 2 * pair + 1] = jnp.where(left, x, 0.0).astype(jnp.bfloat16)

    local[3].wait()
    uc = modulated(context[...], 1)
    kvc = jnp.dot(uc, wkv[...], preferred_element_type=jnp.float32)
    kv_all[0, pl.ds(tokens, ctx_rows), :] = jnp.where(left, headed(kvc, kg), kvc).astype(jnp.bfloat16)
    local[6].wait()
    absorb_rows(latent[...], tp)
    lat[2].wait_recv()
    absorb_rows(raw[0], peers[0])
    lat[3].wait_recv()
    absorb_rows(raw[1], peers[1])
    lat[4].wait_recv()
    lat[5].wait_recv()
    absorb_rows(raw[2], peers[2])

    kvs = {}
    for d in sp_order:
        copy = send(kv_all.at[0], kv_all.at[d], kv_send.at[d - 1], kv_recv.at[d - 1], {"sp": (sp + d) % n_sp})
        copy.start()
        kvs[d] = copy

    factor = LOG2E * HD ** (-0.5)

    def attend(owner, head, slot, first):
        b = owner * group + head
        kv = kv_all[slot]
        s = lax.dot_general(q_all[b], kv, (((1,), (1,)), ((), ())), preferred_element_type=jnp.float32)
        s_lat = s[:, :tokens]
        s_ctx = s[:, tokens:] + lift[head] * (HD ** 0.5)
        m = jnp.maximum(
            jnp.max(s_lat, axis=1, keepdims=True), jnp.max(s_ctx, axis=1, keepdims=True)
        )
        if not first:
            m_old = m_st[b]
            m = jnp.maximum(m, m_old)
        p_lat = jnp.exp2((s_lat - m) * factor)
        p_ctx = jnp.exp2((s_ctx - m) * factor)
        l = jnp.sum(p_lat, axis=1, keepdims=True) + jnp.sum(p_ctx, axis=1, keepdims=True)
        o = jnp.dot(p_lat.astype(jnp.bfloat16), kv[:tokens], preferred_element_type=jnp.float32)
        o = o + jnp.dot(p_ctx.astype(jnp.bfloat16), kv[tokens:], preferred_element_type=jnp.float32)
        if not first:
            alpha = jnp.exp2((m_old - m) * factor)
            l = l + alpha * l_st[b]
            o = o + alpha * acc[b]
        return b, m, l, o

    order = [0] + sp_order
    for step, slot in enumerate(order[:-1]):
        if step > 0:
            kvs[slot].wait_recv()

        def owner_step(owner, carry, slot=slot, step=step):
            for head in range(group):
                b, m, l, o = attend(owner, head, slot, step == 0)
                m_st[b] = m
                l_st[b] = l
                acc[b] = o
            return carry

        lax.fori_loop(0, n_tp, owner_step, 0)

    slot = order[-1]
    kvs[slot].wait_recv()
    span = group * HD
    mine = pl.ds(pl.multiple_of(tp * span, span), span)
    o_copies = []
    for i, owner in enumerate(peers + (tp,)):
        pieces = []
        for head in range(group):
            b, m, l, o = attend(owner, head, slot, False)
            pieces.append((o / l)[:, HD:].astype(jnp.bfloat16))
        joined = jnp.concatenate(pieces, axis=1)
        if i < n_tp - 1:
            o_send[i] = joined
            copy = send(o_send.at[i], o_all.at[:, mine], o_ssem.at[i], o_rsem.at[i], {"tp": owner})
            copy.start()
            o_copies.append(copy)
        else:
            o_all[:, mine] = joined
    local[7].wait()
    for copy in o_copies:
        copy.wait_recv()

    for j in range(n_tp):
        cols = pl.ds(j * chunk, chunk)
        y = jnp.dot(o_all[...], wout[:, cols], preferred_element_type=jnp.float32)
        gate = mods_all[j, 4:5, :]
        out[:, cols] = (latent[:, cols].astype(jnp.float32) + gate * y).astype(jnp.bfloat16)

    for copy in lat + pa + pb + list(kvs.values()) + o_copies:
        copy.wait_send()


def on_device(n_sp, n_tp, latent, cond, cond_ctx, context, norm_gain, mod_shift, mod_scale, mod_gate,
              w_query, w_key, w_value, q_gain, k_gain, ctx_lift, w_out):
    _, rows, width = latent.shape
    tokens = rows * n_tp
    ctx_rows = context.shape[1]
    group = w_query.shape[1] // w_key.shape[1]
    keys = tokens + ctx_rows
    row_tab, col_tab = rope_tables(tokens * n_sp // GRID_W)
    chunk = mod_shift.shape[1]
    bf, f32 = jnp.bfloat16, jnp.float32
    vmem = pl.BlockSpec(memory_space=pltpu.VMEM)
    smem = pl.BlockSpec(memory_space=pltpu.SMEM)
    hbm = pl.BlockSpec(memory_space=pl.ANY)
    dma = pltpu.SemaphoreType.DMA
    out = pl.pallas_call(
        functools.partial(kernel, n_sp, n_tp, group),
        out_shape=jax.ShapeDtypeStruct((rows, width), bf),
        in_specs=[vmem] * 6 + [smem] + [vmem] * 2 + [hbm] * 8,
        out_specs=vmem,
        scratch_shapes=[
            pltpu.VMEM((ctx_rows, width), bf),
            pltpu.VMEM((3,) + mod_shift.shape, bf),
            pltpu.VMEM(w_query.shape, bf),
            pltpu.VMEM(w_key.shape, bf),
            pltpu.VMEM(w_value.shape, bf),
            pltpu.VMEM((width, 2 * HD), bf),
            pltpu.VMEM(w_out.shape, bf),
            pltpu.VMEM((n_tp - 1, rows, width), bf),
            pltpu.VMEM((8, chunk), f32),
            pltpu.VMEM((n_sp - 1, 8, chunk), f32),
            pltpu.VMEM((n_tp, 8, chunk), f32),
            pltpu.VMEM((8, width), f32),
            pltpu.VMEM((2, tokens, 2 * HD), f32),
            pltpu.VMEM((n_tp * group, rows, 2 * HD), bf),
            pltpu.VMEM((n_sp, keys, 2 * HD), bf),
            pltpu.VMEM((n_tp * group, rows, 2 * HD), f32),
            pltpu.VMEM((n_tp * group, rows, 1), f32),
            pltpu.VMEM((n_tp * group, rows, 1), f32),
            pltpu.VMEM((n_tp - 1, rows, group * HD), bf),
            pltpu.VMEM((rows, n_tp * group * HD), bf),
            dma((8,)),
            dma((6,)), dma((6,)),
            dma((n_sp - 1,)), dma((n_sp - 1,)),
            dma((n_tp - 1,)), dma((n_tp - 1,)),
            dma((n_sp - 1,)), dma((n_sp - 1,)),
            dma((n_tp - 1,)), dma((n_tp - 1,)),
        ],
        compiler_params=pltpu.CompilerParams(
            collective_id=0, has_side_effects=True, vmem_limit_bytes=60 * 1024 * 1024
        ),
    )(
        latent[0], cond, cond_ctx[None], norm_gain[None], q_gain[None], k_gain[None], ctx_lift,
        jnp.asarray(row_tab), jnp.asarray(col_tab),
        context[0], mod_shift, mod_scale, mod_gate, w_query, w_key, w_value, w_out,
    )
    return out[None]


def solution(mesh):
    placed = (
        P("dp", ("sp", "tp"), None),
        P("dp", "sp"),
        P("sp"),
        P("dp", "sp", None),
        P(),
        P("sp", "tp"),
        P("sp", "tp"),
        P("sp", "tp"),
        P(None, "tp"),
        P(None, "tp"),
        P(None, "tp"),
        P(),
        P(),
        P("tp"),
        P(),
    )
    return jax.shard_map(
        functools.partial(on_device, mesh.shape["sp"], mesh.shape["tp"]),
        mesh=mesh,
        in_specs=placed,
        out_specs=P("dp", ("sp", "tp"), None),
        check_vma=False,
    )
```

time: 191 us -> 88.9 us (0.47)
  the two profiles are of different devices: /device:TPU:0 before, /device:TPU:18 now
where the time goes in v1:
time: 88.9 us; the launch traced here: 88.6 us
  Pallas kernels  80 us (90%)
  local copies, waits for them, and re-layouts  8.55 us (10%)
    pallas_call x1, Pallas kernels, on_device(): pl.pallas_call(functools.partial(kernel, n_sp, n_tp, group), out_shape=ja...  80 us
    unnamed x3, local copies, waits for them, and re-layouts  6 us

profile of v1, /device:TPU:18, one launch (start us, length us, event | category | flops | bytes accessed | tf_op | source)
XLA Modules:
  0.0 88.6 jit_solution(11890608000261487806)
XLA Ops:
  0.0 1.3 %broadcast_in_dim.15.cond_ctx = bf16[1,512]{1,0:T(2,128)(2,1)} reshape(bf16[512]{0:T(512)(128)(2,1)} %param.19) | data formatting | bytes 2048 | tf_op jit(solution)/shard_map/broadcast_in_dim | solution.py:334
  1.3 1.3 %broadcast_in_dim.16.norm_gain = bf16[1,2048]{1,0:T(2,128)(2,1)} reshape(bf16[2048]{0:T(1024)(128)(2,1)} %param.21) | data formatting | bytes 8192 | tf_op jit(solution)/shard_map/broadcast_in_dim | solution.py:334
  2.6 2.0 %copy.18.wk_h = bf16[2048,64]{1,0:T(8,128)(2,1)} copy(bf16[2048,64]{0,1:T(8,128)(2,1)} %param.26) | data formatting | bytes 524288 | tf_op args[9]
  4.5 2.0 %copy.19.wv_h = bf16[2048,64]{1,0:T(8,128)(2,1)} copy(bf16[2048,64]{0,1:T(8,128)(2,1)} %param.27) | data formatting | bytes 524288 | tf_op args[10]
  6.5 80.0 %shard_map.163 = bf16[192,2048]{1,0:T(8,128)(2,1)} custom-call(bf16[192,2048]{1,0:T(8,128)(2,1)} %bitcast.6, bf16[1,512]{1,0:T(2,128)(2,1)} %cond.1, bf16[1,512]{1,0:T(2,128)(2,1)} %broadcast_in_dim.15.cond_ctx, bf16[1,2048]{1,0:T(2,128)(2,1)} %broadcast_in_dim.16.norm_gain, bf16[1,64]{1,0:T(2,128)(2,1)} %bitcast.8, bf16[1,64]{1,0:T(2,128)(2,1)} %bitcast.9, ...), custom_call_target="tpu_custom_call" | custom-call | tf_op jit(solution)/shard_map/pallas_call | solution.py:297
  86.5 2.1 %copy.21 = bf16[1,192,2048]{2,1,0:T(8,128)(2,1)} copy(bf16[1,192,2048]{2,1,0:T(8,128)(2,1)} %bitcast.5) | data formatting | bytes 1572864

commit v2 on v1

--- a/solution.py
+++ b/solution.py
@@ -14,6 +14,7 @@
 THETA = 10000.0
 MESH = pl.DeviceIdType.MESH
 LOG2E = 1.4426950408889634
+NT = (((1,), (1,)), ((), ()))
 
 
 def rope_tables(grid_rows):
@@ -37,8 +38,8 @@
     latent, cond, cond_ctx, norm_gain, q_gain, k_gain, lift, row_tab, col_tab,
     context_h, mshift_h, mscale_h, mgate_h, wq_h, wk_h, wv_h, wout_h,
     out,
-    context, mods_w, wq, wk, wv, wkv, wout,
-    raw, part, part_in, mods_all, ab, rope, q_all, kv_all, acc, m_st, l_st, o_send, o_all,
+    context, mods_w, wq, wkv, wout,
+    raw, part, part_in, mods_all, ab, rope, q_all, kv_all, kvt, v_one, lift_col, acc, m_st, o_send, o_all,
     local_sem, lat_send, lat_recv, pa_send, pa_recv, pb_send, pb_recv, kv_send, kv_recv, o_ssem, o_rsem,
 ):
     rows = latent.shape[0]
@@ -61,8 +62,8 @@
                 (mscale_h, mods_w.at[1]),
                 (mgate_h, mods_w.at[2]),
                 (context_h, context),
-                (wk_h, wk),
-                (wv_h, wv),
+                (wk_h, wkv.at[pl.ds(0, HD)]),
+                (wv_h, wkv.at[pl.ds(HD, HD)]),
                 (wq_h, wq),
                 (wout_h, wout),
             )
@@ -96,7 +97,7 @@
     send_rows(2, latent.at[low], 0, low, peers[0])
     send_rows(3, latent.at[top], 1, top, peers[1])
 
-    act = jnp.concatenate([cond[...], cond_ctx[...]], axis=0).astype(jnp.float32)
+    act = jnp.concatenate([cond[...], cond_ctx[...].reshape(1, -1)], axis=0).astype(jnp.float32)
     act = (act / (1.0 + jnp.exp(-act))).astype(jnp.bfloat16)
     act = jnp.concatenate([act, jnp.zeros((14, act.shape[1]), jnp.bfloat16)], axis=0)
     for i in range(3):
@@ -115,9 +116,6 @@
             rope[i, pl.ds(g * GRID_W, GRID_W), :] = (
                 row_tab[i, pl.ds(sp * groups + g, 1), :] + col_tab[i, :, :]
             )
-    local[4].wait()
-    local[5].wait()
-    wkv[...] = jnp.concatenate([wk[...], wv[...]], axis=1)
 
     total = part[...]
     for copy in pa:
@@ -137,7 +135,7 @@
 
     for copy in pb:
         copy.wait_recv()
-    gain = norm_gain[...].astype(jnp.float32)
+    gain = norm_gain[...].astype(jnp.float32).reshape(1, -1)
     for j in range(n_tp):
         cols = pl.ds(j * chunk, chunk)
         block = mods_all[j]
@@ -177,21 +175,23 @@
         u = modulated(block, 0)
         where = pl.ds(pl.multiple_of(owner * rows, rows), rows)
         cosine, sine = rope[0, where, :], rope[1, where, :]
-        kv = jnp.dot(u, wkv[...], preferred_element_type=jnp.float32)
+        kv = lax.dot_general(u, wkv[...], NT, preferred_element_type=jnp.float32)
         keys = turned(headed(kv, kg), cosine, sine)
-        kv_all[0, where, :] = jnp.where(left, keys, kv).astype(jnp.bfloat16)
+        kv_all[sp, where, :] = jnp.where(left, keys, kv).astype(jnp.bfloat16)
         raw_q = jnp.dot(u, wq[...], preferred_element_type=jnp.float32)
         for pair in range(group // 2):
             x = raw_q[:, pair * 2 * HD : (pair + 1) * 2 * HD]
             x = turned(headed(x, qg), cosine, sine)
-            q_all[owner * group + 2 * pair] = jnp.where(left, x, 0.0).astype(jnp.bfloat16)
+            q_all[owner, pl.ds(2 * pair * rows, rows), :] = jnp.where(left, x, 0.0).astype(jnp.bfloat16)
             x = pltpu.roll(x, HD, 1)
-            q_all[owner * group + 2 * pair + 1] = jnp.where(left, x, 0.0).astype(jnp.bfloat16)
+            q_all[owner, pl.ds((2 * pair + 1) * rows, rows), :] = jnp.where(left, x, 0.0).astype(jnp.bfloat16)
 
     local[3].wait()
+    local[4].wait()
+    local[5].wait()
     uc = modulated(context[...], 1)
-    kvc = jnp.dot(uc, wkv[...], preferred_element_type=jnp.float32)
-    kv_all[0, pl.ds(tokens, ctx_rows), :] = jnp.where(left, headed(kvc, kg), kvc).astype(jnp.bfloat16)
+    kvc = lax.dot_general(uc, wkv[...], NT, preferred_element_type=jnp.float32)
+    kv_all[sp, pl.ds(tokens, ctx_rows), :] = jnp.where(left, headed(kvc, kg), kvc).astype(jnp.bfloat16)
     local[6].wait()
     absorb_rows(latent[...], tp)
     lat[2].wait_recv()
@@ -202,63 +202,99 @@
     lat[5].wait_recv()
     absorb_rows(raw[2], peers[2])
 
-    kvs = {}
-    for d in sp_order:
-        copy = send(kv_all.at[0], kv_all.at[d], kv_send.at[d - 1], kv_recv.at[d - 1], {"sp": (sp + d) % n_sp})
+    for head in range(group):
+        lift_col[pl.ds(head * rows, rows), :] = jnp.full((rows, 1), lift[head] * (HD ** 0.5), jnp.float32)
+
+    def pass_on(source, side, go):
+        copy = send(
+            kv_all.at[source], kv_all.at[source], kv_send.at[side, source], kv_recv.at[source],
+            {"sp": sp + (1 if side else -1)},
+        )
+        go(copy)
+
+    def start(copy):
         copy.start()
-        kvs[d] = copy
+
+    def spread(source, side, valid):
+        @pl.when(valid & ((sp < n_sp - 1) if side else (sp > 0)))
+        def _():
+            pass_on(source, side, start)
+
+    spread(sp, 1, sp >= 0)
+    spread(sp, 0, sp >= 0)
 
     factor = LOG2E * HD ** (-0.5)
 
-    def attend(owner, head, slot, first):
-        b = owner * group + head
-        kv = kv_all[slot]
-        s = lax.dot_general(q_all[b], kv, (((1,), (1,)), ((), ())), preferred_element_type=jnp.float32)
+    def flip(slot):
+        kv = kv_all[slot].astype(jnp.float32)
+        kvt[...] = kv.T.astype(jnp.bfloat16)
+        v_one[...] = jnp.where(left, 1.0, kv).astype(jnp.bfloat16)
+
+    def attend(owner, slot, first):
+        s = jnp.dot(q_all[owner], kvt[...], preferred_element_type=jnp.float32)
         s_lat = s[:, :tokens]
-        s_ctx = s[:, tokens:] + lift[head] * (HD ** 0.5)
+        s_ctx = s[:, tokens:] + lift_col[...]
         m = jnp.maximum(
             jnp.max(s_lat, axis=1, keepdims=True), jnp.max(s_ctx, axis=1, keepdims=True)
         )
         if not first:
-            m_old = m_st[b]
+            m_old = m_st[owner]
             m = jnp.maximum(m, m_old)
         p_lat = jnp.exp2((s_lat - m) * factor)
         p_ctx = jnp.exp2((s_ctx - m) * factor)
-        l = jnp.sum(p_lat, axis=1, keepdims=True) + jnp.sum(p_ctx, axis=1, keepdims=True)
-        o = jnp.dot(p_lat.astype(jnp.bfloat16), kv[:tokens], preferred_element_type=jnp.float32)
-        o = o + jnp.dot(p_ctx.astype(jnp.bfloat16), kv[tokens:], preferred_element_type=jnp.float32)
+        p = jnp.concatenate([p_lat.astype(jnp.bfloat16), p_ctx.astype(jnp.bfloat16)], axis=1)
+        o = jnp.dot(p, v_one[...], preferred_element_type=jnp.float32)
         if not first:
             alpha = jnp.exp2((m_old - m) * factor)
-            l = l + alpha * l_st[b]
-            o = o + alpha * acc[b]
-        return b, m, l, o
-
-    order = [0] + sp_order
-    for step, slot in enumerate(order[:-1]):
-        if step > 0:
-            kvs[slot].wait_recv()
-
-        def owner_step(owner, carry, slot=slot, step=step):
-            for head in range(group):
-                b, m, l, o = attend(owner, head, slot, step == 0)
-                m_st[b] = m
-                l_st[b] = l
-                acc[b] = o
-            return carry
-
-        lax.fori_loop(0, n_tp, owner_step, 0)
-
-    slot = order[-1]
-    kvs[slot].wait_recv()
+            o = o + alpha * acc[owner]
+        return m, o
+
+    def keep(owner, slot, first):
+        m, o = attend(owner, slot, first)
+        m_st[owner] = m
+        acc[owner] = o
+
+    after = n_sp - 1 - sp
+    near = jnp.minimum(sp, after)
+    toward = jnp.where(sp < after, 1, -1)
+
+    def fetch(k):
+        both = k <= 2 * near
+        distance = jnp.where(both, (k + 1) // 2, k - near)
+        way = jnp.where(both & (k % 2 == 0), -toward, toward)
+
+        @pl.when((k > 2 * near) | (k % 2 == 1))
+        def _():
+            for side in (1, 0):
+                source = (sp - distance) if side else (sp + distance)
+                inside = (source >= 0) if side else (source <= n_sp - 1)
+
+                @pl.when(inside)
+                def _():
+                    pass_on(source, side, lambda copy: copy.wait_recv())
+                    spread(source, side, inside)
+
+        return sp + way * distance
+
+    flip(sp)
+    lax.fori_loop(0, n_tp, lambda owner, c: (keep(owner, sp, True), c)[1], 0)
+
+    def step(k, carry):
+        slot = fetch(k)
+        flip(slot)
+        lax.fori_loop(0, n_tp, lambda owner, c: (keep(owner, slot, False), c)[1], 0)
+        return carry
+
+    lax.fori_loop(1, n_sp - 1, step, 0)
+    slot = fetch(n_sp - 1)
+    flip(slot)
     span = group * HD
     mine = pl.ds(pl.multiple_of(tp * span, span), span)
     o_copies = []
     for i, owner in enumerate(peers + (tp,)):
-        pieces = []
-        for head in range(group):
-            b, m, l, o = attend(owner, head, slot, False)
-            pieces.append((o / l)[:, HD:].astype(jnp.bfloat16))
-        joined = jnp.concatenate(pieces, axis=1)
+        m, o = attend(owner, slot, False)
+        o = (o / pltpu.roll(o, HD, 1)).astype(jnp.bfloat16)
+        joined = jnp.concatenate([o[h * rows : (h + 1) * rows, HD:] for h in range(group)], axis=1)
         if i < n_tp - 1:
             o_send[i] = joined
             copy = send(o_send.at[i], o_all.at[:, mine], o_ssem.at[i], o_rsem.at[i], {"tp": owner})
@@ -276,8 +312,16 @@
         gate = mods_all[j, 4:5, :]
         out[:, cols] = (latent[:, cols].astype(jnp.float32) + gate * y).astype(jnp.bfloat16)
 
-    for copy in lat + pa + pb + list(kvs.values()) + o_copies:
+    for copy in lat + pa + pb + o_copies:
         copy.wait_send()
+    for source in range(n_sp):
+        @pl.when((source <= sp) & (sp < n_sp - 1))
+        def _():
+            pass_on(source, 1, lambda copy: copy.wait_send())
+
+        @pl.when((source >= sp) & (sp > 0))
+        def _():
+            pass_on(source, 0, lambda copy: copy.wait_send())
 
 
 def on_device(n_sp, n_tp, latent, cond, cond_ctx, context, norm_gain, mod_shift, mod_scale, mod_gate,
@@ -303,9 +347,7 @@
             pltpu.VMEM((ctx_rows, width), bf),
             pltpu.VMEM((3,) + mod_shift.shape, bf),
             pltpu.VMEM(w_query.shape, bf),
-            pltpu.VMEM(w_key.shape, bf),
-            pltpu.VMEM(w_value.shape, bf),
-            pltpu.VMEM((width, 2 * HD), bf),
+            pltpu.VMEM((2 * HD, width), bf),
             pltpu.VMEM(w_out.shape, bf),
             pltpu.VMEM((n_tp - 1, rows, width), bf),
             pltpu.VMEM((8, chunk), f32),
@@ -313,27 +355,29 @@
             pltpu.VMEM((n_tp, 8, chunk), f32),
             pltpu.VMEM((8, width), f32),
             pltpu.VMEM((2, tokens, 2 * HD), f32),
-            pltpu.VMEM((n_tp * group, rows, 2 * HD), bf),
+            pltpu.VMEM((n_tp, group * rows, 2 * HD), bf),
             pltpu.VMEM((n_sp, keys, 2 * HD), bf),
-            pltpu.VMEM((n_tp * group, rows, 2 * HD), f32),
-            pltpu.VMEM((n_tp * group, rows, 1), f32),
-            pltpu.VMEM((n_tp * group, rows, 1), f32),
+            pltpu.VMEM((2 * HD, keys), bf),
+            pltpu.VMEM((keys, 2 * HD), bf),
+            pltpu.VMEM((group * rows, 1), f32),
+            pltpu.VMEM((n_tp, group * rows, 2 * HD), f32),
+            pltpu.VMEM((n_tp, group * rows, 1), f32),
             pltpu.VMEM((n_tp - 1, rows, group * HD), bf),
             pltpu.VMEM((rows, n_tp * group * HD), bf),
             dma((8,)),
             dma((6,)), dma((6,)),
             dma((n_sp - 1,)), dma((n_sp - 1,)),
             dma((n_tp - 1,)), dma((n_tp - 1,)),
-            dma((n_sp - 1,)), dma((n_sp - 1,)),
+            dma((2, n_sp)), dma((n_sp,)),
             dma((n_tp - 1,)), dma((n_tp - 1,)),
         ],
         compiler_params=pltpu.CompilerParams(
             collective_id=0, has_side_effects=True, vmem_limit_bytes=60 * 1024 * 1024
         ),
     )(
-        latent[0], cond, cond_ctx[None], norm_gain[None], q_gain[None], k_gain[None], ctx_lift,
+        latent[0], cond, cond_ctx, norm_gain, q_gain[None], k_gain[None], ctx_lift,
         jnp.asarray(row_tab), jnp.asarray(col_tab),
-        context[0], mod_shift, mod_scale, mod_gate, w_query, w_key, w_value, w_out,
+        context[0], mod_shift, mod_scale, mod_gate, w_query, w_key.T, w_value.T, w_out,
     )
     return out[None]
 

time: 88.9 us -> 79.1 us (0.89)
  the two profiles are of different devices: /device:TPU:18 before, /device:TPU:0 now
where the time goes in v2:
time: 79.1 us; the launch traced here: 79 us
  Pallas kernels  76.9 us (97%)
  local copies, waits for them, and re-layouts  2.09 us (3%)
    pallas_call x1, Pallas kernels, on_device(): pl.pallas_call(functools.partial(kernel, n_sp, n_tp, group), out_shape=ja...  76.9 us
    unnamed x1, local copies, waits for them, and re-layouts  2.09 us

profile of v2, /device:TPU:0, one launch (start us, length us, event | category | flops | bytes accessed | tf_op | source)
XLA Modules:
  0.0 79.0 jit_solution(12832549666231282684)
XLA Ops:
  0.0 76.9 %shard_map.163 = bf16[192,2048]{1,0:T(8,128)(2,1)} custom-call(bf16[192,2048]{1,0:T(8,128)(2,1)} %bitcast.8, bf16[1,512]{1,0:T(2,128)(2,1)} %cond.1, bf16[512]{0:T(512)(128)(2,1)} %cond_ctx.1, bf16[2048]{0:T(1024)(128)(2,1)} %norm_gain.1, bf16[1,64]{1,0:T(2,128)(2,1)} %bitcast.12, bf16[1,64]{1,0:T(2,128)(2,1)} %bitcast.13, f32[4]{0:T(128)} %lift.1, ...), custom_call_target="tpu_custom_call" | custom-call | tf_op jit(solution)/shard_map/pallas_call | solution.py:341
  76.9 2.1 %copy.19 = bf16[1,192,2048]{2,1,0:T(8,128)(2,1)} copy(bf16[1,192,2048]{2,1,0:T(8,128)(2,1)} %bitcast.7) | data formatting | bytes 1572864

commit v3 on v2

--- a/solution.py
+++ b/solution.py
@@ -94,8 +94,6 @@
 
     send_rows(0, latent.at[top], 0, top, peers[0])
     send_rows(1, latent.at[low], 1, low, peers[1])
-    send_rows(2, latent.at[low], 0, low, peers[0])
-    send_rows(3, latent.at[top], 1, top, peers[1])
 
     act = jnp.concatenate([cond[...], cond_ctx[...].reshape(1, -1)], axis=0).astype(jnp.float32)
     act = (act / (1.0 + jnp.exp(-act))).astype(jnp.bfloat16)
@@ -128,6 +126,8 @@
         copy = send(mods_all.at[tp], mods_all.at[tp], pb_send.at[i], pb_recv.at[i], {"tp": peer})
         copy.start()
         pb.append(copy)
+    send_rows(2, latent.at[low], 0, low, peers[0])
+    send_rows(3, latent.at[top], 1, top, peers[1])
     lat[0].wait_recv()
     send_rows(4, raw.at[0, top], 2, top, peers[1])
     lat[1].wait_recv()

time: 79.1 us -> 79.1 us (level)
  no operation moved by 1% of the time
where the time goes in v3:
time: 79.1 us; the launch traced here: 79 us
  Pallas kernels  76.9 us (97%)
  local copies, waits for them, and re-layouts  2.09 us (3%)
    pallas_call x1, Pallas kernels, on_device(): pl.pallas_call(functools.partial(kernel, n_sp, n_tp, group), out_shape=ja...  76.9 us
    unnamed x1, local copies, waits for them, and re-layouts  2.09 us

profile of v3, /device:TPU:0, one launch (start us, length us, event | category | flops | bytes accessed | tf_op | source)
XLA Modules:
  0.0 79.0 jit_solution(305717354456389814)
XLA Ops:
  0.0 76.9 %shard_map.163 = bf16[192,2048]{1,0:T(8,128)(2,1)} custom-call(bf16[192,2048]{1,0:T(8,128)(2,1)} %bitcast.8, bf16[1,512]{1,0:T(2,128)(2,1)} %cond.1, bf16[512]{0:T(512)(128)(2,1)} %cond_ctx.1, bf16[2048]{0:T(1024)(128)(2,1)} %norm_gain.1, bf16[1,64]{1,0:T(2,128)(2,1)} %bitcast.12, bf16[1,64]{1,0:T(2,128)(2,1)} %bitcast.13, f32[4]{0:T(128)} %lift.1, ...), custom_call_target="tpu_custom_call" | custom-call | tf_op jit(solution)/shard_map/pallas_call | solution.py:341
  76.9 2.1 %copy.19 = bf16[1,192,2048]{2,1,0:T(8,128)(2,1)} copy(bf16[1,192,2048]{2,1,0:T(8,128)(2,1)} %bitcast.7) | data formatting | bytes 1572864
